TPU v7x, 256 devices: a 4x2x16 block of a 4x16x16 slice. The times are simulated.
256 devices in a mesh: grp: 2 (over y), sp: 32 (over z, core), tp: 4 (over x).
Axes of the slice: x: 4, y: 2, z: 16, core: 2. Of those that a mesh axis runs over, the one named last changes fastest.
The devices are a block of a 4x16x16 slice.
Arguments:
- query_first: bfloat16 [12288, 512], P(('grp', 'sp'), 'tp'), parts along dimension 0, may hold values from -172 to 172
- key_first: bfloat16 [12288, 512], P(('grp', 'sp'), 'tp'), parts along dimension 0, may hold values from -7.8 to 7.8
- query_second: bfloat16 [12288, 1024], P(('grp', 'sp'), 'tp'), parts along dimension 0, may hold values from -172 to 172
- key_second: bfloat16 [12288, 1024], P(('grp', 'sp'), 'tp'), parts along dimension 0, may hold values from -7.8 to 7.8
- values: bfloat16 [12288, 2, 512], P(('grp', 'sp'), None, 'tp'), parts along dimension 0, may hold values from -6 to 6
- lambdas: float32 [2, 4], P(None, 'tp'), may hold values from 0.3 to 0.8
- residual: bfloat16 [12288, 2048], P(('grp', 'sp'), 'tp'), parts along dimension 0, may hold values from -130 to 130
- norm_gain: bfloat16 [2048], P('tp'), may hold values from 0.099609375 to 1.8984375
- out_weight: bfloat16 [2, 512, 2048], P(None, 'tp'), may hold values from -0.1875 to 0.1875
- gate_weight: bfloat16 [2048, 5632], P('sp', 'tp'), may hold values from -0.125 to 0.125
- up_weight: bfloat16 [2048, 5632], P('sp', 'tp'), may hold values from -0.125 to 0.125
- down_weight: bfloat16 [5632, 2048], P('tp', 'sp'), may hold values from -0.078125 to 0.078125
Outputs:
- layer_out: bfloat16 [12288, 2048], P(('grp', 'sp'), 'tp'), parts along dimension 0
There are 2 independent parts, one for each index of `grp`. A program takes and returns all parts, laid end to end along the dimension named above; an argument that names none is the same for every part. Nothing has to cross between parts.
All inputs are finite; a program needn't handle non-finite values.
Results may differ from a plain program's by a relative error of at most 0.0065.
Values may be sent and summed in bfloat16 or wider, within the bound.
A program may use at most 128 MiB of HBM per device.

v0:
```python
import math

import jax
import jax.numpy as jnp
from jax import lax
from jax.sharding import PartitionSpec as P

D = 2048


def side_by_side(arrays, axis, dim, along):
    widths = [math.prod(a.shape[along:]) for a in arrays]
    both = jnp.concatenate(
        [a.reshape(*a.shape[:along], w) for a, w in zip(arrays, widths)], axis=along
    )
    out = lax.all_gather(both, axis, axis=dim, tiled=True)
    blocks = jnp.split(out, [sum(widths[:k]) for k in range(1, len(widths))], axis=along)
    return tuple((b.reshape(*out.shape[:along], *a.shape[along:]) for a, b in zip(arrays, blocks)))


def split_up(shard, dim, count):
    lengths = shard.shape
    blocks = shard.reshape(*lengths[:dim], count, lengths[dim] // count, *lengths[dim + 1 :])
    return jnp.moveaxis(blocks, dim, 0)


def sum_at_owner(shard, axis, dim):
    count = lax.axis_size(axis)
    blocks = lax.all_to_all(split_up(shard, dim, count), axis, 0, 0, tiled=True)
    return jnp.sum(blocks.astype(jnp.float32), axis=0)


def from_everyone(shard, axis):
    copies = jnp.broadcast_to(shard, (lax.axis_size(axis), *shard.shape))
    return lax.all_to_all(copies, axis, split_axis=0, concat_axis=0, tiled=True)


def taken_together(shard, axis):
    everything = from_everyone(shard, axis)
    return jnp.sum(everything, axis=0)


def joined_along(blocks, dim):
    lengths = list(blocks.shape[1:])
    lengths[dim] *= blocks.shape[0]
    return jnp.moveaxis(blocks, 0, dim).reshape(lengths)


def gathered_copies(shard, axis, dim):
    blocks = from_everyone(shard, axis)
    return joined_along(blocks, dim)


def sent_together(arrays, axis, dim, along):
    ends, at = ([], 0)
    for a in arrays[:-1]:
        at += a.shape[along]
        ends.append(at)
    both = jnp.concatenate(arrays, axis=along)
    return tuple(jnp.split(lax.all_gather(both, axis, axis=dim, tiled=True), ends, axis=along))


def per_device(
    query_first,
    key_first,
    query_second,
    key_second,
    values,
    lambdas,
    residual,
    norm_gain,
    out_weight,
    gate_weight,
    up_weight,
    down_weight,
):
    tok_rows = query_first.shape[0]
    heads_here = lambdas.shape[1]
    width_first = query_first.shape[1] // (2 * heads_here)
    width_second = query_second.shape[1] // (2 * heads_here)
    value_size = values.shape[2] // heads_here
    offset = lax.axis_index("sp") * tok_rows
    query_pos = offset + lax.broadcasted_iota(jnp.int32, (tok_rows, 1), 0)
    query_groups = (
        query_first.reshape(tok_rows, heads_here, 2, width_first),
        query_second.reshape(tok_rows, heads_here, 2, width_second),
    )
    key_widths = (width_first, width_second)
    start_state = (
        jnp.full((heads_here, 2, tok_rows, 1), -1e30, jnp.float32),
        jnp.zeros((heads_here, 2, tok_rows, 1), jnp.float32),
        jnp.zeros((heads_here, 2, tok_rows, value_size), jnp.float32),
    )
    states = (start_state, start_state)
    pieces = side_by_side((key_first, key_second, values), "sp", 0, 1)
    piece_rows = pieces[0].shape[0]
    key_pos = lax.broadcasted_iota(jnp.int32, (1, piece_rows), 1)
    allowed = key_pos <= query_pos
    value_rows = pieces[2].reshape(piece_rows, 2, heads_here, value_size)
    results = []
    for group_idx in range(2):
        key_width = key_widths[group_idx]
        key_part = pieces[group_idx].reshape(piece_rows, heads_here, 2, key_width)
        scores = jnp.einsum(
            "qhmd,khmd->hmqk", query_groups[group_idx], key_part, preferred_element_type=jnp.float32
        ) * key_width ** (-0.5)
        scores = jnp.where(allowed, scores, -1e30)
        running, totals, weighted = states[group_idx]
        new_peak = jnp.maximum(running, jnp.max(scores, axis=-1, keepdims=True))
        weights = jnp.where(allowed, jnp.exp(scores - new_peak), 0.0)
        totals = jnp.sum(weights, axis=-1, keepdims=True)
        weighted = jnp.einsum(
            "hmqk,khe->hmqe",
            weights.astype(jnp.bfloat16),
            value_rows[:, group_idx],
            preferred_element_type=jnp.float32,
        )
        results.append((new_peak, totals, weighted))
    states = (results[0], results[1])
    map_out = jnp.stack([states[0][2] / states[0][1], states[1][2] / states[1][1]])
    differ = map_out[:, :, 0] - lambdas[:, :, None, None] * map_out[:, :, 1]
    head_scale = lax.rsqrt(jnp.mean(differ * differ, axis=-1, keepdims=True) + 1e-06)
    attended = (0.8 * differ * head_scale).astype(jnp.bfloat16)
    projection = out_weight.reshape(2, heads_here, value_size, out_weight.shape[2])
    mixed_part = jnp.einsum(
        "ghqe,gher->qr", attended, projection, preferred_element_type=jnp.float32
    )
    mixed = sum_at_owner(mixed_part.astype(jnp.bfloat16), "tp", 1)
    stream = residual.astype(jnp.float32) + mixed
    squares = taken_together(jnp.sum(stream * stream, axis=1), "tp")
    row_scale = lax.rsqrt(squares[:, None] / D + 1e-06)
    normed = (stream * row_scale * norm_gain.astype(jnp.float32)).astype(jnp.bfloat16)
    full_rows = gathered_copies(normed, "tp", 1)
    pieces = sent_together((gate_weight, up_weight), "sp", 0, 1)
    gate = jnp.dot(full_rows, pieces[0], preferred_element_type=jnp.float32)
    up_part = jnp.dot(full_rows, pieces[1], preferred_element_type=jnp.float32)
    hidden = (jax.nn.silu(gate) * up_part).astype(jnp.bfloat16)
    partial_out = jnp.dot(
        hidden,
        lax.all_gather(down_weight, "sp", axis=1, tiled=True),
        preferred_element_type=jnp.float32,
    )
    ffn = sum_at_owner(partial_out.astype(jnp.bfloat16), "tp", 1)
    return (stream + 0.5 * ffn).astype(jnp.bfloat16)


def solution(mesh):
    return jax.shard_map(
        per_device,
        mesh=mesh,
        in_specs=(
            P(("grp", "sp"), "tp"),
            P(("grp", "sp"), "tp"),
            P(("grp", "sp"), "tp"),
            P(("grp", "sp"), "tp"),
            P(("grp", "sp"), None, "tp"),
            P(None, "tp"),
            P(("grp", "sp"), "tp"),
            P("tp"),
            P(None, "tp", None),
            P("sp", "tp"),
            P("sp", "tp"),
            P("tp", "sp"),
        ),
        out_specs=P(("grp", "sp"), "tp"),
        check_vma=False,
    )
```

profile of v0, /device:TPU:34, one launch (start us, length us, event | category | flops | bytes accessed | tf_op | source)
XLA Modules:
  0.0 283.5 jit_solution(16304569291432327499)
XLA Ops:
  6.6 1.0 copy.86
  7.6 1.6 pad_maximum_fusion.1
  9.3 1.8 pad_maximum_fusion
  12.0 0.9 copy.51
  13.7 86.0 %all-gather.4.cloned.1.call-done = bf16[6144,640]{1,0:T(8,128)(2,1)} async-done(((bf16[192,640]{1,0:T(8,128)(2,1)}), bf16[6144,640]{1,0:T(8,128)(2,1)}) %all-gather.4.cloned.1.call-update) | async-done | bytes 7864336 | tf_op jit(solution)/shard_map/all_gather | solution.py:16
  99.6 6.0 %fusion.55 = (bf16[6144,256]{1,0:T(8,128)(2,1)}, bf16[6144,256]{1,0:T(8,128)(2,1)}) fusion(bf16[6144,640]{1,0:T(8,128)(2,1)} %all-gather.4.cloned.1.call-done), kind=kLoop, calls=%fused_computation.69 | loop fusion | bytes 12582912 | tf_op jit(solution)/shard_map/split | solution.py:17
  105.6 4.7 %copy.67 = bf16[6144,256]{0,1:T(8,128)(2,1)} copy(bf16[6144,256]{1,0:T(8,128)(2,1)} %get-tuple-element.7) | data formatting | bytes 6291456
  110.3 2.7 split.20
  113.0 2.6 copy.50
  115.7 4.7 %copy.65 = bf16[6144,256]{0,1:T(8,128)(2,1)} copy(bf16[6144,256]{1,0:T(8,128)(2,1)} %get-tuple-element.8) | data formatting | bytes 6291456
  120.4 3.8 %fusion.57 = (f32[2,192]{1,0:T(2,128)S(1)}, f32[2,192,6144]{2,1,0:T(8,128)S(1)}) fusion(bf16[6144,2,64]{0,2,1:T(8,128)(2,1)} %bitcast.106, bf16[192,2,64]{0,2,1:T(8,128)(2,1)S(1)} %bitcast.112, pred[192,6144]{1,0:T(8,128)(4,1)S(1)} %iota_compare_fusion), kind=kOutput, calls=%fused_computation.71 | convolution fusion | flops 309067392 | bytes 12240384 | tf_op jit(solution)/shard_map/qhmd,khmd->hmqk/dot_general | solution.py:104
  124.2 2.6 fusion.56
  126.9 4.5 %fusion = (f32[2,192]{1,0:T(2,128)S(1)}, f32[2,192]{1,0:T(2,128)S(1)}) fusion(f32[2,192,6144]{2,1,0:T(8,128)S(1)} %get-tuple-element.12, f32[2,192]{1,0:T(2,128)S(1)} %get-tuple-element.14, pred[192,6144]{1,0:T(8,128)(4,1)S(1)} %iota_compare_fusion, f32[2,192,6144]{2,1,0:T(8,128)S(1)} %get-tuple-element.10, f32[2,192]{1,0:T(2,128)S(1)} %get-tuple-element.13), kind=kLoop, calls=%fused_computation.4 | loop fusion | flops 14155008 | bytes 20060160 | tf_op jit(solution)/shard_map/reduce_sum | solution.py:111
  131.4 2.1 fusion.36
  133.6 2.1 fusion.30
  136.5 15.8 %all_to_all.21 = bf16[4,192,512]{2,1,0:T(8,128)(2,1)S(1)} all-to-all(bf16[4,192,512]{2,1,0:T(8,128)(2,1)S(1)} %bitcast.103), channel_id=1, replica_groups=mesh['grp'=2,'sp'=32,'tp'=4] {'tp'}, dimensions={0} | all-to-all | bytes 1572864 | tf_op jit(solution)/shard_map/all_to_all | solution.py:29
  153.2 4.7 %all-to-all-start.1 = ((f32[4,1,192]{2,1,0:T(1,128)}), f32[4,1,192]{2,1,0:T(1,128)S(1)}, u32[]{:S(2)}, u32[]{:S(2)}) async-start(f32[4,1,192]{2,1,0:T(1,128)} %broadcast_in_dim.37), calls=%async_computation.1 | async-start | bytes 8192 | tf_op jit(solution)/shard_map/all_to_all | solution.py:35
  157.9 3.9 %all-to-all-done.1 = f32[4,1,192]{2,1,0:T(1,128)S(1)} async-done(((f32[4,1,192]{2,1,0:T(1,128)}), f32[4,1,192]{2,1,0:T(1,128)S(1)}, u32[]{:S(2)}, u32[]{:S(2)}) %all-to-all-start.1) | async-done | bytes 3104 | tf_op jit(solution)/shard_map/all_to_all | solution.py:35
  162.0 13.2 %all_to_all.22 = bf16[4,192,512]{2,1,0:T(8,128)(2,1)S(1)} all-to-all(bf16[4,192,512]{2,1,0:T(8,128)(2,1)S(1)} %broadcast_in_dim.38), channel_id=1, replica_groups=mesh['grp'=2,'sp'=32,'tp'=4] {'tp'}, dimensions={0} | all-to-all | bytes 1572864 | tf_op jit(solution)/shard_map/all_to_all | solution.py:35
  175.3 5.1 %all-gather.6.cloned.1.call-done = bf16[2048,2816]{1,0:T(8,128)(2,1)} async-done(((bf16[64,2816]{1,0:T(8,128)(2,1)}), bf16[2048,2816]{1,0:T(8,128)(2,1)}) %all-gather.6.cloned.1.call-update) | async-done | bytes 11534352 | tf_op jit(solution)/shard_map/all_gather | solution.py:60
  180.4 5.0 %fusion.6 = f32[192,1408]{1,0:T(8,128)} fusion(bf16[192,2048]{1,0:T(8,128)(2,1)S(1)} %bitcast.107, bf16[2048,2816]{1,0:T(8,128)(2,1)} %all-gather.6.cloned.1.call-done), kind=kOutput, calls=%fused_computation.10 | convolution fusion | flops 1107296256 | bytes 7634944 | tf_op jit(solution)/shard_map/dot_general | solution.py:135
  185.4 67.0 %all-gather.8.cloned.1.call-done = bf16[1408,2048]{0,1:T(8,128)(2,1)} async-done(((bf16[1408,64]{0,1:T(8,128)(2,1)}), bf16[1408,2048]{0,1:T(8,128)(2,1)}) %all-gather.8.cloned.1.call-update) | async-done | bytes 5767184 | tf_op jit(solution)/shard_map/all_gather | solution.py:140
  252.4 7.9 %convolution_convert_fusion = bf16[192,2048]{1,0:T(8,128)(2,1)S(1)} fusion(bf16[1408,2048]{0,1:T(8,128)(2,1)} %all-gather.8.cloned.1.call-done, bf16[192,2048]{1,0:T(8,128)(2,1)S(1)} %bitcast.108, bf16[2048,2816]{1,0:T(8,128)(2,1)} %all-gather.6.cloned.1.call-done, f32[192,1408]{1,0:T(8,128)} %fusion.6), kind=kOutput, calls=%fused_computation.25 | convolution fusion | flops 2216607744 | bytes 14188544 | tf_op jit(solution)/shard_map/dot_general | solution.py:138
  260.4 15.7 %all_to_all.23 = bf16[4,192,512]{2,1,0:T(8,128)(2,1)S(1)} all-to-all(bf16[4,192,512]{2,1,0:T(8,128)(2,1)S(1)} %bitcast.105), channel_id=1, replica_groups=mesh['grp'=2,'sp'=32,'tp'=4] {'tp'}, dimensions={0} | all-to-all | bytes 1572864 | tf_op jit(solution)/shard_map/all_to_all | solution.py:29
  (39 shorter events, 4.6 us)
Async XLA Ops:
  6.5 129.4 %copy-start = (bf16[2,128,2048]{2,1,0:T(8,128)(2,1)S(1)}, bf16[2,128,2048]{2,1,0:T(8,128)(2,1)}, u32[]{:S(2)}) copy-start(bf16[2,128,2048]{2,1,0:T(8,128)(2,1)} %param.20) | copy-start | bytes 3145732
  6.6 93.1 %all-gather.4.cloned.1.call-start = ((), (), s32[]{:S(2)}) async-start(), calls=%async_computation.4 | async-start | bytes 8110080 | tf_op jit(solution)/shard_map/all_gather | solution.py:16
  9.2 171.1 %all-gather.6.cloned.1.call-start = ((), (), s32[]{:S(2)}) async-start(), calls=%async_computation.5 | async-start | bytes 11894784 | tf_op jit(solution)/shard_map/all_gather | solution.py:60
  11.2 241.2 %all-gather.8.cloned.1.call-start = ((), (), s32[]{:S(2)}) async-start(), calls=%async_computation.6 | async-start | bytes 5947392 | tf_op jit(solution)/shard_map/all_gather | solution.py:140
  120.4 3.8 %copy-start.1 = (bf16[6144,256]{0,1:T(8,128)(2,1)S(1)}, bf16[6144,256]{0,1:T(8,128)(2,1)}, u32[]{:S(2)}) copy-start(bf16[6144,256]{0,1:T(8,128)(2,1)} %copy.67) | copy-start | bytes 9437188
  120.4 3.8 %copy-start.4 = (bf16[192,256]{1,0:T(8,128)(2,1)S(1)}, bf16[192,256]{1,0:T(8,128)(2,1)}, u32[]{:S(2)}) copy-start(bf16[192,256]{1,0:T(8,128)(2,1)} %param.14) | copy-start | bytes 294916
  126.8 4.6 %copy-start.2 = (bf16[6144,256]{0,1:T(8,128)(2,1)S(1)}, bf16[6144,256]{0,1:T(8,128)(2,1)}, u32[]{:S(2)}) copy-start(bf16[6144,256]{0,1:T(8,128)(2,1)} %copy.65) | copy-start | bytes 9437188
  133.6 2.2 copy-start.5
  135.7 16.7 %copy-start.3 = (bf16[192,512]{1,0:T(8,128)(2,1)S(1)}, bf16[192,512]{1,0:T(8,128)(2,1)}, u32[]{:S(2)}) copy-start(bf16[192,512]{1,0:T(8,128)(2,1)} %param.18) | copy-start | bytes 589828
  135.7 22.1 %copy-start.6 = (bf16[512]{0:T(512)(128)(2,1)S(1)}, bf16[512]{0:T(512)(128)(2,1)}, u32[]{:S(2)}) copy-start(bf16[512]{0:T(512)(128)(2,1)} %param.19) | copy-start | bytes 3076
  153.2 8.6 %all-to-all-start.1 = ((f32[4,1,192]{2,1,0:T(1,128)}), f32[4,1,192]{2,1,0:T(1,128)S(1)}, u32[]{:S(2)}, u32[]{:S(2)}) async-start(f32[4,1,192]{2,1,0:T(1,128)} %broadcast_in_dim.37), calls=%async_computation.1 | async-start | bytes 8192 | tf_op jit(solution)/shard_map/all_to_all | solution.py:35
Sparse Core Ops, SparseCore 0:
  9.4 90.2 all-gather.3
  101.5 78.8 all-gather.5
  182.2 70.0 all-gather.7
where the time goes:
time: 285 us; the launch traced here: 284 us
  waiting for transfers between devices  163 us (57%)
  blocking collectives  44.8 us (16%)
  matrix products  24.1 us (8%)
  local copies, waits for them, and re-layouts  23.5 us (8%)
  between operations  13.4 us (5%)
  other arithmetic  10.2 us (4%)
  starting transfers between devices  4.82 us (2%)
    all_gather x1, waiting for transfers between devices, side_by_side(): out = lax.all_gather(both, axis, axis=dim, tiled=True)  86 us
    all_gather x1, waiting for transfers between devices, per_device(): lax.all_gather(down_weight, 'sp', axis=1, tiled=True)  67 us
    all_to_all x2, blocking collectives, sum_at_owner(): blocks = lax.all_to_all(split_up(shard, dim, count), axis, 0, 0, tiled=True)  31.6 us
    all_to_all x1, blocking collectives, from_everyone(): return lax.all_to_all(copies, axis, split_axis=0, concat_axis=0, tiled=True)  13.2 us
    split x3, local copies, waits for them, and re-layouts, side_by_side(): jnp.split(out, [sum(widths[:k]) for k in range(1, len(widths))], axis=along)  11.3 us
    unnamed x18, local copies, waits for them, and re-layouts  11.3 us
    dot_general x1, matrix products, per_device(): jnp.dot(hidden, lax.all_gather(down_weight, 'sp', axis=1, tiled=True), pr...  7.92 us
    dot_general x2, matrix products, per_device(): jnp.einsum('qhmd,khmd->hmqk', query_groups[group_idx], key_part, preferre...  6.44 us
  transfers between devices with their start and end apart: 4, of which 4 were waited for; matrix products, arithmetic and copies ran while one was open for 16% of the time, Pallas kernels for 0%

commit v1 on v0

v1 whole, which is shorter than its diff:
```python
import functools
import math

import jax
import jax.numpy as jnp
from jax import lax
from jax.experimental import pallas as pl
from jax.experimental.pallas import tpu as pltpu
from jax.sharding import PartitionSpec as P

MESH = pl.DeviceIdType.MESH
F32 = jnp.float32
BF16 = jnp.bfloat16
NT_DIMS = (((1,), (1,)), ((), ()))


class Ring:
    def __init__(self, index, buf, rows, start, size, across=None):
        self.index, self.buf, self.rows = index, buf, rows
        self.start, self.size, self.across = start, size, across


def kernel(
    nz, nt, lam_ref, q1_ref, q2_ref, gain_ref, kv_hbm, res_hbm, ow_hbm, gate_hbm, up_hbm, down_hbm,
    out_ref,
    kv, gate, up, down, ow, res, qa, qb, m_ref, l_ref, acc_ref, att, mix_send, mix_recv, mix_own,
    stream, sq, xg, hid, ffn_send, ffn_recv,
    zs, zr, ds, dr, ys, yr, es, er, xs, xr, local,
):
    g, s, t = lax.axis_index("grp"), lax.axis_index("sp"), lax.axis_index("tp")
    z, c = s // 2, s % 2
    half = nz // 2
    rows = res.shape[0]
    pair = 2 * rows
    feat = res.shape[1]
    wrows = gate_hbm.shape[0]
    part = g % 2
    sign = 1 - 2 * c

    def wrap(v):
        return lax.rem(v + 2 * nz, nz)

    def chip(v):
        return (g, 2 * wrap(v) + c, t)

    partner = (g, s + sign, t)
    across = (g + 1 - 2 * part, s, t)

    def other(k):
        return lax.rem(t + k, nt)

    own_kv = pl.ds(pl.multiple_of(rows * s, 16), rows)
    own_w = pl.ds(pl.multiple_of(wrows * s, 16), wrows)
    loads = [
        pltpu.make_async_copy(kv_hbm, kv.at[own_kv, :], local.at[0]),
        pltpu.make_async_copy(gate_hbm, gate.at[own_w, :], local.at[1]),
        pltpu.make_async_copy(up_hbm, up.at[own_w, :], local.at[2]),
        pltpu.make_async_copy(down_hbm, down.at[own_w, :], local.at[3]),
        pltpu.make_async_copy(ow_hbm, ow, local.at[4]),
        pltpu.make_async_copy(res_hbm, res, local.at[5]),
    ]
    for load in loads:
        load.start()
    barrier = pltpu.get_barrier_semaphore()
    peers = [chip(z + 1), chip(z - 1), partner, across] + [(g, s, other(k)) for k in range(1, nt)]
    for peer in peers:
        pl.semaphore_signal(barrier, inc=1, device_id=peer, device_id_type=MESH)

    w1, w2 = q1_ref.shape[1], q2_ref.shape[1]
    lane1 = lax.broadcasted_iota(jnp.int32, (rows, w1), 1)
    lane2 = lax.broadcasted_iota(jnp.int32, (rows, w2), 1)
    q1, q2 = q1_ref[...], q2_ref[...]
    qa[pl.ds(0, rows), :] = jnp.where(lane1 < w1 // 2, q1, jnp.zeros_like(q1))
    qa[pl.ds(rows, rows), :] = jnp.where(lane1 < w1 // 2, jnp.zeros_like(q1), q1)
    qb[pl.ds(0, rows), :] = jnp.where(lane2 < w2 // 2, q2, jnp.zeros_like(q2))
    qb[pl.ds(rows, rows), :] = jnp.where(lane2 < w2 // 2, jnp.zeros_like(q2), q2)

    pl.semaphore_wait(barrier, len(peers))

    def view(ring, slot, start=None, size=None):
        start = ring.start if start is None else start
        size = ring.size if size is None else size
        return ring.buf.at[pl.ds(pl.multiple_of(ring.rows * slot + start, 16), size), :]

    def remote(ref, send, recv, device):
        return pltpu.make_async_remote_copy(
            src_ref=ref, dst_ref=ref, send_sem=send, recv_sem=recv, device_id=device, device_id_type=MESH
        )

    def at_distance(way, d):
        return wrap(z - d) if way == 0 else wrap(z + d)

    def onward(ring, way, d):
        n = ring.index
        ref = view(ring, 2 * at_distance(way, d) + c)
        return remote(ref, zs.at[n, way, d], zr.at[n, way, d + 1], chip(z + 1 - 2 * way))

    def arrived(ring, way, d):
        n = ring.index
        ref = view(ring, 2 * at_distance(way, d) + c)
        return remote(ref, zs.at[n, way, d], zr.at[n, way, d], chip(z + 1 - 2 * way))

    def last_onward(ring):
        n = ring.index
        ref = view(ring, 2 * wrap(z - (half - 1) * sign) + c)
        return remote(ref, zs.at[n, 0, half - 1], zr.at[n, 0, half], chip(z + sign))

    def to_partner(ring, way, d):
        n = ring.index
        return remote(view(ring, 2 * at_distance(way, d) + c), ds.at[n, way, d], dr.at[n, way, d], partner)

    def from_partner(ring, way, d):
        n = ring.index
        ref = view(ring, 2 * at_distance(way, d) + 1 - c)
        return remote(ref, ds.at[n, way, d], dr.at[n, way, d], partner)

    def own_to_partner(ring, core):
        n = ring.index
        whole = ring.across is not None
        start, size = (0, ring.rows) if whole else (ring.start, ring.size)
        return remote(view(ring, 2 * z + core, start, size), ds.at[n, 0, 0], dr.at[n, 0, 0], partner)

    def to_across(ring, way, d):
        n = ring.across
        return remote(view(ring, 2 * at_distance(way, d) + c), ys.at[n, way, d], yr.at[n, way, d], across)

    def other_half(ring):
        return ring.size * (1 - part)

    def from_across(ring, way, d):
        n = ring.across
        ref = view(ring, 2 * at_distance(way, d) + c, other_half(ring))
        return remote(ref, ys.at[n, way, d], yr.at[n, way, d], across)

    def across_to_partner(ring, way, d, core):
        n = ring.across
        ref = view(ring, 2 * at_distance(way, d) + core, other_half(ring))
        return remote(ref, es.at[n, way, d], er.at[n, way, d], partner)

    def begin(rings):
        for ring in rings:
            for way in range(2):
                onward(ring, way, 0).start()
        for ring in rings:
            own_to_partner(ring, c).start()

    def landed(ring, way, d):
        arrived(ring, way, d).wait_recv()

    def pass_on(ring, way, d):
        to_partner(ring, way, d).start()
        if ring.across is not None:
            to_across(ring, way, d).start()

    def take_across(ring, way, d):
        from_across(ring, way, d).wait_recv()
        across_to_partner(ring, way, d, c).start()

    def turn(rings, then):
        def step(d, carry):
            for ring in rings:
                for way in range(2):
                    landed(ring, way, d)

                    @pl.when(d < half - 1)
                    def _():
                        onward(ring, way, d).start()

                    pass_on(ring, way, d)

                    if ring.across is not None:

                        @pl.when(d > 1)
                        def _():
                            take_across(ring, way, d - 1)

            @pl.when(d == half - 1)
            def _():
                for ring in rings:
                    last_onward(ring).start()

            then(d)
            return carry

        lax.fori_loop(1, half, step, 0)

    def turn_end(rings):
        for ring in rings:
            landed(ring, 0, half)
            pass_on(ring, 0, half)

    def finish_across(rings):
        for ring in rings:
            if ring.across is not None:
                for way in range(2):
                    take_across(ring, way, half - 1)
                take_across(ring, 0, half)

    def settle_partner(rings):
        for ring in rings:
            own_to_partner(ring, 1 - c).wait_recv()

            def step(d, carry):
                for way in range(2):
                    from_partner(ring, way, d).wait_recv()
                    if ring.across is not None:
                        across_to_partner(ring, way, d, 1 - c).wait_recv()
                return carry

            lax.fori_loop(1, half, step, 0)
            from_partner(ring, 0, half).wait_recv()
            if ring.across is not None:
                across_to_partner(ring, 0, half, 1 - c).wait_recv()

    def settle_sends(rings):
        for ring in rings:

            def step(d, carry):
                for way in range(2):
                    onward(ring, way, d - 1).wait_send()
                    to_partner(ring, way, d).wait_send()
                    if ring.across is not None:
                        to_across(ring, way, d).wait_send()
                        across_to_partner(ring, way, d, c).wait_send()
                return carry

            lax.fori_loop(1, half, step, 0)
            last_onward(ring).wait_send()
            own_to_partner(ring, c).wait_send()
            to_partner(ring, 0, half).wait_send()
            if ring.across is not None:
                to_across(ring, 0, half).wait_send()
                across_to_partner(ring, 0, half, c).wait_send()

    cut = rows // 2
    kv_rings = [Ring(0, kv, rows, 0, cut), Ring(1, kv, rows, cut, cut)]
    gate_ring = Ring(2, gate, wrows, 0, wrows)
    up_ring = Ring(3, up, wrows, (wrows // 2) * part, wrows // 2, across=0)
    down_ring = Ring(4, down, wrows, (wrows // 2) * part, wrows // 2, across=1)

    value_size = acc_ref.shape[2]
    log2e = 1.4426950408889634
    k_cols = ((0, w1), (w1, w2))
    v_at = w1 + w2

    def attend(zk, first):
        at = pl.ds(pl.multiple_of(pair * zk, 16), pair)
        for group in range(2):
            q_ref = (qa, qb)[group]
            col, width = k_cols[group]
            factor = (width // 2) ** (-0.5) * log2e
            scores = lax.dot_general(
                q_ref[...], kv[at, pl.ds(col, width)], NT_DIMS, preferred_element_type=F32
            )
            if first:
                q_at = lax.broadcasted_iota(jnp.int32, (pair, pair), 0)
                k_at = lax.broadcasted_iota(jnp.int32, (pair, pair), 1)
                q_at = jnp.where(q_at >= rows, q_at - rows, q_at) + rows * c
                scores = jnp.where(k_at <= q_at, scores, -1e30)
            peak = jnp.max(scores, axis=1, keepdims=True)
            if not first:
                old = m_ref[group][:, :1]
                peak = jnp.maximum(old, peak)
                alpha = jnp.exp2((old - peak) * factor)
            weights = jnp.exp2((scores - peak) * factor)
            total = jnp.sum(weights, axis=1, keepdims=True)
            values = kv[at, pl.ds(v_at + group * value_size, value_size)]
            out = jnp.dot(weights.astype(BF16), values, preferred_element_type=F32)
            if not first:
                total = total + alpha * l_ref[group][:, :1]
                out = out + alpha * acc_ref[group]
            m_ref[group] = jnp.broadcast_to(peak, (pair, 128))
            l_ref[group] = jnp.broadcast_to(total, (pair, 128))
            acc_ref[group] = out

    def attend_step(d):
        def one(i, carry):
            zk = jnp.where(i == 0, z - d, z + d - nz)

            @pl.when(zk >= 0)
            def _():
                attend(zk, False)

            return carry

        lax.fori_loop(0, 2, one, 0)

    def swap(ref_from, ref_to, which, k):
        return pltpu.make_async_remote_copy(
            src_ref=ref_from, dst_ref=ref_to, send_sem=xs.at[which, k - 1], recv_sem=xr.at[which, k - 1],
            device_id=(g, s, other(k)), device_id_type=MESH,
        )

    def mine(which, k):
        if which == 0:
            return swap(mix_send.at[k - 1], mix_recv.at[k - 1], 0, k)
        if which == 1:
            cols = xg.at[:, pl.ds(pl.multiple_of(feat * t, 128), feat)]
            return swap(cols, cols, 1, k)
        if which == 2:
            return swap(sq.at[t], sq.at[t], 2, k)
        return swap(ffn_send.at[k - 1], ffn_recv.at[k - 1], 3, k)

    def theirs(which, k):
        frm = lax.rem(t + nt - k, nt)
        if which == 1:
            cols = xg.at[:, pl.ds(pl.multiple_of(feat * frm, 128), feat)]
            return swap(cols, cols, 1, k)
        if which == 2:
            return swap(sq.at[frm], sq.at[frm], 2, k)
        return mine(which, k)

    loads[0].wait()
    begin(kv_rings)
    for load in loads[1:4]:
        load.wait()
    ffn_rings = [gate_ring, up_ring]

    def kv_then(d):
        @pl.when(d == 1)
        def _():
            for ring in kv_rings:
                own_to_partner(ring, 1 - c).wait_recv()
            attend(z, True)

        @pl.when(d == half - 2)
        def _():
            begin(ffn_rings)

        @pl.when(d > 1)
        def _():
            for ring in kv_rings:
                for way in range(2):
                    from_partner(ring, way, d - 1).wait_recv()
            attend_step(d - 1)

    turn(kv_rings, kv_then)
    turn_end(kv_rings)
    for ring in kv_rings:
        for way in range(2):
            from_partner(ring, way, half - 1).wait_recv()
    attend_step(half - 1)
    for ring in kv_rings:
        from_partner(ring, 0, half).wait_recv()

    @pl.when(z >= half)
    def _():
        attend(z - half, False)

    for group in range(2):
        map_out = acc_ref[group] / l_ref[group]
        differ = map_out[:rows] - lam_ref[group, 0] * map_out[rows:]
        scale = lax.rsqrt(jnp.mean(differ * differ, axis=1, keepdims=True) + 1e-06)
        att[:, pl.ds(group * value_size, value_size)] = (0.8 * differ * scale).astype(BF16)
    loads[4].wait()
    for k in range(1, nt):
        cols = pl.ds(pl.multiple_of(feat * other(k), 128), feat)
        mix_send[k - 1] = jnp.dot(att[...], ow[:, cols], preferred_element_type=F32).astype(BF16)
    mix_own[...] = jnp.dot(
        att[...], ow[:, pl.ds(pl.multiple_of(feat * t, 128), feat)], preferred_element_type=F32
    )
    for k in range(1, nt):
        mine(0, k).start()
    loads[5].wait()

    def ffn_then(d):
        @pl.when(d == 3)
        def _():
            total = mix_own[...] + res[...].astype(F32)
            for k in range(1, nt):
                theirs(0, k).wait_recv()
                total = total + mix_recv[k - 1].astype(F32)
            stream[...] = total
            sq[t] = jnp.broadcast_to(jnp.sum(total * total, axis=1, keepdims=True), sq.shape[1:])
            xg[:, pl.ds(pl.multiple_of(feat * t, 128), feat)] = (
                total * gain_ref[...].astype(F32)
            ).astype(BF16)

        @pl.when(d == 4)
        def _():
            for k in range(1, nt):
                mine(1, k).start()
                mine(2, k).start()

        @pl.when(d == half - 2)
        def _():
            begin([down_ring])

    turn(ffn_rings, ffn_then)
    turn_end(ffn_rings)
    finish_across(ffn_rings)
    settle_partner(ffn_rings)
    for k in range(1, nt):
        theirs(1, k).wait_recv()
        theirs(2, k).wait_recv()
    squares = sq[0]
    for k in range(1, nt):
        squares = squares + sq[k]
    model = feat * nt
    row_scale = lax.rsqrt(squares / model + 1e-06)[:, :1]
    m_ref[0, pl.ds(0, rows), :] = jnp.broadcast_to(row_scale, (rows, 128))

    hidden = hid.shape[1]
    tile = 256

    def hidden_tile(cols):
        scale = m_ref[0, pl.ds(0, rows), :][:, :1]
        gates = jnp.dot(xg[...], gate[:, cols], preferred_element_type=F32) * scale
        ups = jnp.dot(xg[...], up[:, cols], preferred_element_type=F32) * scale
        hid[:, cols] = (gates / (1.0 + jnp.exp(-gates)) * ups).astype(BF16)

    tiles, rest = hidden // tile, hidden % tile

    def down_then(d):
        @pl.when(d <= tiles)
        def _():
            hidden_tile(pl.ds(pl.multiple_of((d - 1) * tile, 128), tile))

        @pl.when(d == tiles + 1)
        def _():
            hidden_tile(pl.ds(tiles * tile, rest))

    turn([down_ring], down_then)
    turn_end([down_ring])
    finish_across([down_ring])
    settle_partner([down_ring])

    def share(owner):
        parts = []
        for i in range(2):
            at = pl.ds(pl.multiple_of(feat * owner + i * (feat // 2), 16), feat // 2)
            parts.append(lax.dot_general(hid[...], down[at, :], NT_DIMS, preferred_element_type=F32))
        return jnp.concatenate(parts, axis=1)

    for k in (2, 1, 3):
        ffn_send[k - 1] = share(other(k)).astype(BF16)
    own = share(t)
    for k in (2, 1, 3):
        mine(3, k).start()
    settle_sends(kv_rings + ffn_rings + [down_ring])
    for which in range(3):
        for k in range(1, nt):
            mine(which, k).wait_send()
    for k in range(1, nt):
        theirs(3, k).wait_recv()
        own = own + ffn_recv[k - 1].astype(F32)
    out_ref[...] = (stream[...] + 0.5 * own).astype(BF16)
    for k in range(1, nt):
        mine(3, k).wait_send()


def layer(
    nz, nt, query_first, key_first, query_second, key_second, values, lambdas, residual, norm_gain,
    out_weight, gate_weight, up_weight, down_weight,
):
    rows, feat = residual.shape
    wrows, hidden = gate_weight.shape
    value_size = values.shape[2]
    model = feat * nt
    kv = jnp.concatenate([key_first, key_second, values.reshape(rows, -1)], axis=1)
    w1, w2 = query_first.shape[1], query_second.shape[1]
    any_ref = pl.BlockSpec(memory_space=pltpu.HBM)
    vmem = pl.BlockSpec(memory_space=pltpu.VMEM)
    half = nz // 2
    dma = pltpu.SemaphoreType.DMA
    return pl.pallas_call(
        functools.partial(kernel, nz, nt),
        out_shape=jax.ShapeDtypeStruct((rows, feat), BF16),
        in_specs=[pl.BlockSpec(memory_space=pltpu.SMEM), vmem, vmem, vmem] + [any_ref] * 6,
        out_specs=vmem,
        scratch_shapes=[
            pltpu.VMEM((2 * nz * rows, kv.shape[1]), BF16),
            pltpu.VMEM((2 * nz * wrows, hidden), BF16),
            pltpu.VMEM((2 * nz * wrows, hidden), BF16),
            pltpu.VMEM((2 * nz * wrows, hidden), BF16),
            pltpu.VMEM((2 * value_size, model), BF16),
            pltpu.VMEM((rows, feat), BF16),
            pltpu.VMEM((2 * rows, w1), BF16),
            pltpu.VMEM((2 * rows, w2), BF16),
            pltpu.VMEM((2, 2 * rows, 128), F32),
            pltpu.VMEM((2, 2 * rows, 128), F32),
            pltpu.VMEM((2, 2 * rows, value_size), F32),
            pltpu.VMEM((rows, 2 * value_size), BF16),
            pltpu.VMEM((nt - 1, rows, feat), BF16),
            pltpu.VMEM((nt - 1, rows, feat), BF16),
            pltpu.VMEM((rows, feat), F32),
            pltpu.VMEM((rows, feat), F32),
            pltpu.VMEM((nt, rows, 128), F32),
            pltpu.VMEM((rows, model), BF16),
            pltpu.VMEM((rows, hidden), BF16),
            pltpu.VMEM((nt - 1, rows, feat), BF16),
            pltpu.VMEM((nt - 1, rows, feat), BF16),
            dma((5, 2, half + 1)),
            dma((5, 2, half + 1)),
            dma((5, 2, half + 1)),
            dma((5, 2, half + 1)),
            dma((2, 2, half + 1)),
            dma((2, 2, half + 1)),
            dma((2, 2, half + 1)),
            dma((2, 2, half + 1)),
            dma((4, nt - 1)),
            dma((4, nt - 1)),
            dma((6,)),
        ],
        compiler_params=pltpu.CompilerParams(
            collective_id=0, has_side_effects=True, vmem_limit_bytes=60 * 2**20
        ),
    )(
        lambdas, query_first, query_second, norm_gain.reshape(1, feat), kv, residual,
        out_weight.reshape(2 * value_size, model), gate_weight, up_weight, down_weight.T,
    )


def solution(mesh):
    return jax.shard_map(
        functools.partial(layer, mesh.shape["sp"] // 2, mesh.shape["tp"]),
        mesh=mesh,
        in_specs=(
            P(("grp", "sp"), "tp"),
            P(("grp", "sp"), "tp"),
            P(("grp", "sp"), "tp"),
            P(("grp", "sp"), "tp"),
            P(("grp", "sp"), None, "tp"),
            P(None, "tp"),
            P(("grp", "sp"), "tp"),
            P("tp"),
            P(None, "tp", None),
            P("sp", "tp"),
            P("sp", "tp"),
            P("tp", "sp"),
        ),
        out_specs=P(("grp", "sp"), "tp"),
        check_vma=False,
    )
```

time: 285 us -> 187 us (0.66)
  Pallas kernels: 0 us -> 179 us
  waiting for transfers between devices: 163 us -> 0 us
  blocking collectives: 44.8 us -> 0 us
  matrix products: 24.1 us -> 0 us
  local copies, waits for them, and re-layouts: 23.5 us -> 4.48 us
  between operations: 13.4 us -> 0.03 us
  other arithmetic: 10.2 us -> 0.71 us
  starting transfers between devices: 4.82 us -> 0 us
    pallas_call x0 -> x1, Pallas kernels: none -> 179 us  [layer(): pl.pallas_call(functools.partial(kernel, nz, nt), out_shape=jax.ShapeDtyp...]
    all_gather x3 -> x0, waiting for transfers between devices: 158 us -> none  [the longest x1 86 us: side_by_side(): out = lax.all_gather(both, axis, axis=dim, tiled=True)]
    all_to_all x3 -> x0, blocking collectives: 44.8 us -> none  [the longest x2 31.6 us: sum_at_owner(): blocks = lax.all_to_all(split_up(shard, dim, count), axis, 0, 0, tiled=True)]
    dot_general x7 -> x0, matrix products: 24.1 us -> none  [the longest x1 7.92 us: per_device(): jnp.dot(hidden, lax.all_gather(down_weight, 'sp', axis=1, tiled=True), pr...]
    split x3 -> x0, local copies, waits for them, and re-layouts: 11.3 us -> none  [side_by_side(): jnp.split(out, [sum(widths[:k]) for k in range(1, len(widths))], axis=along)]
    unnamed x18 -> x11, local copies, waits for them, and re-layouts: 11.3 us -> 3.9 us
    reduce_sum x6 -> x0, other arithmetic: 5.12 us -> none  [the longest x1 4.54 us: per_device(): totals = jnp.sum(weights, axis=-1, keepdims=True)]
    all_to_all x1 -> x0, starting transfers between devices: 4.69 us -> none  [from_everyone(): return lax.all_to_all(copies, axis, split_axis=0, concat_axis=0, tiled=True)]
  transfers between devices with their start and end apart: 4 -> 0, of which waited for: 4 -> 0; matrix products, arithmetic and copies ran while one was open for 16% -> 0% of each run, Pallas kernels for 0% -> 0%
where the time goes in v1:
time: 187 us; the launch traced here: 184 us
  Pallas kernels  179 us (96%)
  local copies, waits for them, and re-layouts  4.48 us (2%)
    pallas_call x1, Pallas kernels, layer(): pl.pallas_call(functools.partial(kernel, nz, nt), out_shape=jax.ShapeDtyp...  179 us
    unnamed x11, local copies, waits for them, and re-layouts  3.9 us

profile of v1, /device:TPU:34, one launch (start us, length us, event | category | flops | bytes accessed | tf_op | source)
XLA Modules:
  0.0 184.2 jit_solution(10363910144032206412)
XLA Ops:
  0.0 0.0 copy-start.3
  0.0 0.7 copy-done.3
  0.7 0.0 copy-start.2
  0.7 0.6 copy.13.lam_ref
  1.3 0.0 copy-done.2
  1.3 0.6 reshape.9.gain_ref
  1.9 0.0 copy-start
  1.9 0.0 copy-start.1
  1.9 0.9 copy.16
  2.9 0.0 copy-done
  2.9 0.0 copy-done.1
  2.9 0.7 pad_maximum_fusion.kv_hbm
  3.6 179.0 %shard_map.118 = bf16[192,512]{1,0:T(8,128)(2,1)} custom-call(f32[2,1]{1,0:T(2,128)} %copy.13.lam_ref, bf16[192,128]{1,0:T(8,128)(2,1)} %q1_ref.1, bf16[192,256]{1,0:T(8,128)(2,1)} %q2_ref.1, bf16[1,512]{1,0:T(2,128)(2,1)} %reshape.9.gain_ref, bf16[192,640]{1,0:T(8,128)(2,1)} %pad_maximum_fusion.kv_hbm, bf16[192,512]{1,0:T(8,128)(2,1)} %res_hbm.1, ...), custom_call_target="tpu_custom_call" | custom-call | tf_op jit(solution)/shard_map/pallas_call | solution.py:466
  182.6 1.6 copy.18
Async XLA Ops:
  0.0 0.7 copy-start.3
  0.7 0.7 copy-start.2
  1.9 0.9 copy-start
  1.9 1.0 copy-start.1

commit v2 on v1

v2 whole, which is shorter than its diff:
```python
import functools
import math

import jax
import jax.numpy as jnp
from jax import lax
from jax.experimental import pallas as pl
from jax.experimental.pallas import tpu as pltpu
from jax.sharding import PartitionSpec as P

MESH = pl.DeviceIdType.MESH
F32 = jnp.float32
BF16 = jnp.bfloat16
NT_DIMS = (((1,), (1,)), ((), ()))
SPLIT = 16


class Ring:
    def __init__(self, index, buf, rows, low, size, across=None):
        self.index, self.buf, self.rows = index, buf, rows
        self.low, self.size, self.across = low, size, across


def kernel(
    nz, nt, lam_ref, q1_ref, q2_ref, gain_ref, k1_hbm, k2_hbm, v_hbm, res_hbm, ow_hbm, gate_hbm, up_hbm, down_hbm,
    out_ref,
    kv, gate, up, down, ow, res, qa, qb, m_ref, l_ref, acc_ref, att, mix_send, mix_recv, mix_own,
    stream, sq, xg, hid, ffn_send, ffn_recv, ffn_own,
    sent, zr, dr, yr, er, xs, xr, local,
):
    g, s, t = lax.axis_index("grp"), lax.axis_index("sp"), lax.axis_index("tp")
    z, c = s // 2, s % 2
    half = nz // 2
    rows = res.shape[0]
    pair = 2 * rows
    feat = res.shape[1]
    wrows = gate_hbm.shape[0]
    part = g % 2
    sign = 1 - 2 * c

    def wrap(v):
        return lax.rem(v + 2 * nz, nz)

    def chip(v):
        return (g, 2 * wrap(v) + c, t)

    partner = (g, s + sign, t)
    across = (g + 1 - 2 * part, s, t)

    def other(k):
        return lax.rem(t + k, nt)

    own_kv = pl.ds(pl.multiple_of(rows * s, 16), rows)
    own_w = pl.ds(pl.multiple_of(wrows * s, 16), wrows)
    k1_width, k2_width, v_width = k1_hbm.shape[1], k2_hbm.shape[1], v_hbm.shape[1]
    loads = [
        pltpu.make_async_copy(k1_hbm, kv.at[own_kv, pl.ds(0, k1_width)], local.at[0]),
        pltpu.make_async_copy(k2_hbm, kv.at[own_kv, pl.ds(k1_width, k2_width)], local.at[1]),
        pltpu.make_async_copy(v_hbm, kv.at[own_kv, pl.ds(k1_width + k2_width, v_width)], local.at[2]),
        pltpu.make_async_copy(up_hbm, up.at[own_w, :], local.at[3]),
        pltpu.make_async_copy(gate_hbm, gate.at[own_w, :], local.at[4]),
        pltpu.make_async_copy(down_hbm, down.at[own_w, :], local.at[5]),
        pltpu.make_async_copy(ow_hbm, ow, local.at[6]),
        pltpu.make_async_copy(res_hbm, res, local.at[7]),
    ]
    for load in loads:
        load.start()
    barrier = pltpu.get_barrier_semaphore()
    peers = [chip(z + 1), chip(z - 1), partner, across] + [(g, s, other(k)) for k in range(1, nt)]
    for peer in peers:
        pl.semaphore_signal(barrier, inc=1, device_id=peer, device_id_type=MESH)

    w1, w2 = q1_ref.shape[1], q2_ref.shape[1]
    lane1 = lax.broadcasted_iota(jnp.int32, (rows, w1), 1)
    lane2 = lax.broadcasted_iota(jnp.int32, (rows, w2), 1)
    q1, q2 = q1_ref[...], q2_ref[...]
    qa[pl.ds(0, rows), :] = jnp.where(lane1 < w1 // 2, q1, jnp.zeros_like(q1))
    qa[pl.ds(rows, rows), :] = jnp.where(lane1 < w1 // 2, jnp.zeros_like(q1), q1)
    qb[pl.ds(0, rows), :] = jnp.where(lane2 < w2 // 2, q2, jnp.zeros_like(q2))
    qb[pl.ds(rows, rows), :] = jnp.where(lane2 < w2 // 2, jnp.zeros_like(q2), q2)

    pl.semaphore_wait(barrier, len(peers))

    def view(ring, slot, start, size):
        return ring.buf.at[pl.ds(pl.multiple_of(ring.rows * slot + start, 8), size), :]

    def of_mine(ring, slot):
        shift = 0 if ring.across is None else ring.size * part
        return view(ring, slot, ring.low + shift, ring.size)

    def of_across(ring, slot):
        return view(ring, slot, ring.low + ring.size * (1 - part), ring.size)

    def remote(ring, ref, recv, device):
        return pltpu.make_async_remote_copy(
            src_ref=ref, dst_ref=ref, send_sem=sent.at[ring.index], recv_sem=recv,
            device_id=device, device_id_type=MESH,
        )

    def total(ring, count, recv):
        return remote(ring, ring.buf.at[pl.ds(0, count * ring.size), :], recv, partner)

    def at_distance(way, d):
        return 2 * (wrap(z - d) if way == 0 else wrap(z + d))

    def onward(ring, way, d):
        ref = of_mine(ring, at_distance(way, d) + c)
        return remote(ring, ref, zr.at[ring.index, way, d + 1], chip(z + 1 - 2 * way))

    def landed(ring, way, d):
        ref = of_mine(ring, at_distance(way, d) + c)
        remote(ring, ref, zr.at[ring.index, way, d], partner).wait_recv()

    def last_onward(ring):
        ref = of_mine(ring, 2 * wrap(z - (half - 1) * sign) + c)
        return remote(ring, ref, zr.at[ring.index, 0, half], chip(z + sign))

    def begin(rings):
        for ring in rings:
            for way in range(2):
                onward(ring, way, 0).start()
        for ring in rings:
            size = ring.size if ring.across is None else 2 * ring.size
            ref = view(ring, 2 * z + c, ring.low, size)
            remote(ring, ref, dr.at[ring.index, 0], partner).start()

    def pass_on(ring, way, d):
        ref = of_mine(ring, at_distance(way, d) + c)
        if ring.across is not None:
            remote(ring, ref, yr.at[ring.across, way, d], across).start()
        remote(ring, ref, dr.at[ring.index, d], partner).start()

    def take_across(ring, way, d):
        ref = of_across(ring, at_distance(way, d) + c)
        remote(ring, ref, yr.at[ring.across, way, d], across).wait_recv()
        remote(ring, ref, er.at[ring.across, d], partner).start()

    def from_partner(ring, d, count):
        if ring.across is not None:
            total(ring, 2 if count == 0 else count, dr.at[ring.index, d]).wait_recv()
            if count > 0:
                total(ring, count, er.at[ring.across, d]).wait_recv()
        else:
            total(ring, 1 if count == 0 else count, dr.at[ring.index, d]).wait_recv()

    def all_from_partner(rings):
        for ring in rings:
            from_partner(ring, 0, 0)

            def step(d, carry):
                from_partner(ring, d, 2)
                return carry

            lax.fori_loop(1, half, step, 0)
            from_partner(ring, half, 1)

    def turn(rings, then):
        def step(d, carry):
            for ring in rings:
                for way in range(2):
                    landed(ring, way, d)

                    @pl.when(d < half - 1)
                    def _():
                        onward(ring, way, d).start()

                    pass_on(ring, way, d)

                    if ring.across is not None:

                        @pl.when(d > 1)
                        def _():
                            take_across(ring, way, d - 1)

            @pl.when(d == half - 1)
            def _():
                for ring in rings:
                    last_onward(ring).start()

            then(d)
            return carry

        lax.fori_loop(1, half, step, 0)

    def turn_end(rings):
        for ring in rings:
            landed(ring, 0, half)
            pass_on(ring, 0, half)

    def finish_across(rings):
        for ring in rings:
            if ring.across is not None:
                for way in range(2):
                    take_across(ring, way, half - 1)
                take_across(ring, 0, half)

    def all_sent(rings):
        for ring in rings:
            count = 4 * half - 1 if ring.across is None else 8 * half - 2
            total(ring, count, dr.at[ring.index, 0]).wait_send()

    cut = rows // 2
    kv_rings = [Ring(0, kv, rows, 0, cut), Ring(1, kv, rows, cut, cut)]
    up_rings = [Ring(2, up, wrows, 0, wrows // 2, across=0)]
    gate_rings = [
        Ring(3, gate, wrows, 0, SPLIT, across=1), Ring(4, gate, wrows, 2 * SPLIT, wrows - 2 * SPLIT)
    ]
    down_rings = [
        Ring(5, down, wrows, 0, SPLIT, across=2), Ring(6, down, wrows, 2 * SPLIT, wrows - 2 * SPLIT)
    ]

    value_size = acc_ref.shape[2]
    log2e = 1.4426950408889634
    k_cols = ((0, w1), (w1, w2))
    v_at = w1 + w2

    def attend(zk, first):
        at = pl.ds(pl.multiple_of(pair * zk, 16), pair)
        for group in range(2):
            q_ref = (qa, qb)[group]
            col, width = k_cols[group]
            factor = (width // 2) ** (-0.5) * log2e
            scores = lax.dot_general(
                q_ref[...], kv[at, pl.ds(col, width)], NT_DIMS, preferred_element_type=F32
            )
            if first:
                q_at = lax.broadcasted_iota(jnp.int32, (pair, pair), 0)
                k_at = lax.broadcasted_iota(jnp.int32, (pair, pair), 1)
                q_at = jnp.where(q_at >= rows, q_at - rows, q_at) + rows * c
                scores = jnp.where(k_at <= q_at, scores, -1e30)
            peak = jnp.max(scores, axis=1, keepdims=True)
            if not first:
                old = m_ref[group][:, :1]
                peak = jnp.maximum(old, peak)
                alpha = jnp.exp2((old - peak) * factor)
            weights = jnp.exp2((scores - peak) * factor)
            total = jnp.sum(weights, axis=1, keepdims=True)
            values = kv[at, pl.ds(v_at + group * value_size, value_size)]
            out = jnp.dot(weights.astype(BF16), values, preferred_element_type=F32)
            if not first:
                total = total + alpha * l_ref[group][:, :1]
                out = out + alpha * acc_ref[group]
            m_ref[group] = jnp.broadcast_to(peak, (pair, 128))
            l_ref[group] = jnp.broadcast_to(total, (pair, 128))
            acc_ref[group] = out

    def attend_step(d):
        def one(i, carry):
            zk = jnp.where(i == 0, z - d, z + d - nz)

            @pl.when(zk >= 0)
            def _():
                attend(zk, False)

            return carry

        lax.fori_loop(0, 2, one, 0)

    def swap(ref_from, ref_to, which, k):
        return pltpu.make_async_remote_copy(
            src_ref=ref_from, dst_ref=ref_to, send_sem=xs.at[which, k - 1], recv_sem=xr.at[which, k - 1],
            device_id=(g, s, other(k)), device_id_type=MESH,
        )

    def mine(which, k):
        if which == 0:
            return swap(mix_send.at[k - 1], mix_recv.at[k - 1], 0, k)
        if which == 1:
            cols = xg.at[:, pl.ds(pl.multiple_of(feat * t, 128), feat)]
            return swap(cols, cols, 1, k)
        if which == 2:
            return swap(sq.at[t], sq.at[t], 2, k)
        return swap(ffn_send.at[k - 1], ffn_recv.at[k - 1], 3, k)

    def theirs(which, k):
        frm = lax.rem(t + nt - k, nt)
        if which == 1:
            cols = xg.at[:, pl.ds(pl.multiple_of(feat * frm, 128), feat)]
            return swap(cols, cols, 1, k)
        if which == 2:
            return swap(sq.at[frm], sq.at[frm], 2, k)
        return mine(which, k)

    for load in loads[:3]:
        load.wait()
    begin(kv_rings)
    loads[3].wait()
    begin(up_rings)
    for load in loads[4:6]:
        load.wait()

    def kv_then(d):
        @pl.when(d == 1)
        def _():
            for ring in kv_rings:
                from_partner(ring, 0, 0)
            attend(z, True)

        @pl.when(d == half - 2)
        def _():
            begin(gate_rings)

        @pl.when(d > 1)
        def _():
            for ring in kv_rings:
                from_partner(ring, d - 1, 2)
            attend_step(d - 1)

    turn(kv_rings + up_rings, kv_then)
    turn_end(kv_rings + up_rings)
    for ring in kv_rings:
        from_partner(ring, half - 1, 2)
    attend_step(half - 1)
    for ring in kv_rings:
        from_partner(ring, half, 1)

    @pl.when(z >= half)
    def _():
        attend(z - half, False)

    for group in range(2):
        map_out = acc_ref[group] / l_ref[group]
        differ = map_out[:rows] - lam_ref[0, group] * map_out[rows:]
        scale = lax.rsqrt(jnp.mean(differ * differ, axis=1, keepdims=True) + 1e-06)
        att[:, pl.ds(group * value_size, value_size)] = (0.8 * differ * scale).astype(BF16)
    loads[6].wait()
    order = (2, 1, 3)
    for k in order:
        cols = pl.ds(pl.multiple_of(feat * other(k), 128), feat)
        mix_send[k - 1] = jnp.dot(att[...], ow[:, cols], preferred_element_type=F32).astype(BF16)
    mix_own[...] = jnp.dot(
        att[...], ow[:, pl.ds(pl.multiple_of(feat * t, 128), feat)], preferred_element_type=F32
    )
    for k in order:
        mine(0, k).start()
    loads[7].wait()

    def gate_then(d):
        @pl.when(d == 4)
        def _():
            acc = mix_own[...] + res[...].astype(F32)
            for k in order:
                theirs(0, k).wait_recv()
                acc = acc + mix_recv[k - 1].astype(F32)
            stream[...] = acc
            sq[t] = jnp.broadcast_to(jnp.sum(acc * acc, axis=1, keepdims=True), sq.shape[1:])
            xg[:, pl.ds(pl.multiple_of(feat * t, 128), feat)] = (
                acc * gain_ref[...].astype(F32)
            ).astype(BF16)
            for k in order:
                mine(1, k).start()
                mine(2, k).start()

        @pl.when(d == half - 2)
        def _():
            begin(down_rings)

    finish_across(up_rings)
    turn(gate_rings, gate_then)
    turn_end(gate_rings)
    all_from_partner(up_rings)

    hidden = hid.shape[1]
    tile = 256

    def hidden_tile(cols):
        scale = m_ref[0, pl.ds(0, rows), :][:, :1]
        gates = jnp.dot(xg[...], gate[:, cols], preferred_element_type=F32) * scale
        ups = jnp.dot(xg[...], up[:, cols], preferred_element_type=F32) * scale
        hid[:, cols] = (gates / (1.0 + jnp.exp(-gates)) * ups).astype(BF16)

    tiles, rest = hidden // tile, hidden % tile

    def hidden_units():
        finish_across(gate_rings)
        all_from_partner(gate_rings)
        for k in order:
            theirs(1, k).wait_recv()
            theirs(2, k).wait_recv()
        squares = sq[0]
        for k in range(1, nt):
            squares = squares + sq[k]
        m_ref[0, pl.ds(0, rows), :] = lax.rsqrt(squares / (feat * nt) + 1e-06)

        def one(i, carry):
            hidden_tile(pl.ds(pl.multiple_of(i * tile, 128), tile))
            return carry

        lax.fori_loop(0, tiles, one, 0)
        hidden_tile(pl.ds(tiles * tile, rest))

    def share(owner):
        parts = []
        for i in range(2):
            at = pl.ds(pl.multiple_of(feat * owner + i * (feat // 2), 16), feat // 2)
            parts.append(lax.dot_general(hid[...], down[at, :], NT_DIMS, preferred_element_type=F32))
        return jnp.concatenate(parts, axis=1)

    def give(owner):
        value = share(owner)
        k = lax.rem(owner - t + nt, nt)

        @pl.when(k == 0)
        def _():
            ffn_own[...] = value

        @pl.when(k > 0)
        def _():
            ffn_send[k - 1] = value.astype(BF16)
            mine(3, k).start()

    chips = nz // nt
    here, place = z // chips, lax.rem(z, chips)

    def near(v):
        return lax.rem(here + v + nt, nt)

    def down_then(d):
        @pl.when(d == 1)
        def _():
            for ring in down_rings:
                from_partner(ring, 0, 0)

        @pl.when(d > 1)
        def _():
            for ring in down_rings:
                from_partner(ring, d - 1, 2)

        @pl.when(d == 2)
        def _():
            hidden_units()

        ready = (d == chips) | (d == chips + 1 + place) | (d == 2 * chips - place)

        @pl.when(ready)
        def _():
            give(jnp.where(d == chips, here, jnp.where(d == chips + 1 + place, near(-1), near(1))))

    turn(down_rings, down_then)
    turn_end(down_rings)
    finish_across(down_rings)
    for ring in down_rings:
        from_partner(ring, half - 1, 2)

    @pl.when((place == 0) | (place == chips - 1))
    def _():
        give(jnp.where(place == 0, near(1), near(-1)))

    for ring in down_rings:
        from_partner(ring, half, 1)
    give(near(2))
    all_sent(kv_rings + up_rings + gate_rings + down_rings)
    for which in range(3):
        for k in range(1, nt):
            mine(which, k).wait_send()
    acc = ffn_own[...]
    for k in range(1, nt):
        theirs(3, k).wait_recv()
        acc = acc + ffn_recv[k - 1].astype(F32)
    out_ref[...] = (stream[...] + 0.5 * acc).astype(BF16)
    for k in range(1, nt):
        mine(3, k).wait_send()


def layer(
    nz, nt, query_first, key_first, query_second, key_second, values, lambdas, residual, norm_gain,
    out_weight, gate_weight, up_weight, down_weight,
):
    rows, feat = residual.shape
    wrows, hidden = gate_weight.shape
    value_size = values.shape[2]
    model = feat * nt
    kv_width = key_first.shape[1] + key_second.shape[1] + 2 * value_size
    w1, w2 = query_first.shape[1], query_second.shape[1]
    any_ref = pl.BlockSpec(memory_space=pltpu.HBM)
    vmem = pl.BlockSpec(memory_space=pltpu.VMEM)
    half = nz // 2
    dma = pltpu.SemaphoreType.DMA
    return pl.pallas_call(
        functools.partial(kernel, nz, nt),
        out_shape=jax.ShapeDtypeStruct((rows, feat), BF16),
        in_specs=[pl.BlockSpec(memory_space=pltpu.SMEM), vmem, vmem, vmem] + [any_ref] * 8,
        out_specs=vmem,
        scratch_shapes=[
            pltpu.VMEM((2 * nz * rows, kv_width), BF16),
            pltpu.VMEM((2 * nz * wrows, hidden), BF16),
            pltpu.VMEM((2 * nz * wrows, hidden), BF16),
            pltpu.VMEM((2 * nz * wrows, hidden), BF16),
            pltpu.VMEM((2 * value_size, model), BF16),
            pltpu.VMEM((rows, feat), BF16),
            pltpu.VMEM((2 * rows, w1), BF16),
            pltpu.VMEM((2 * rows, w2), BF16),
            pltpu.VMEM((2, 2 * rows, 128), F32),
            pltpu.VMEM((2, 2 * rows, 128), F32),
            pltpu.VMEM((2, 2 * rows, value_size), F32),
            pltpu.VMEM((rows, 2 * value_size), BF16),
            pltpu.VMEM((nt - 1, rows, feat), BF16),
            pltpu.VMEM((nt - 1, rows, feat), BF16),
            pltpu.VMEM((rows, feat), F32),
            pltpu.VMEM((rows, feat), F32),
            pltpu.VMEM((nt, rows, 128), F32),
            pltpu.VMEM((rows, model), BF16),
            pltpu.VMEM((rows, hidden), BF16),
            pltpu.VMEM((nt - 1, rows, feat), BF16),
            pltpu.VMEM((nt - 1, rows, feat), BF16),
            pltpu.VMEM((rows, feat), F32),
            dma((7,)),
            dma((7, 2, half + 1)),
            dma((7, half + 1)),
            dma((3, 2, half + 1)),
            dma((3, half + 1)),
            dma((4, nt - 1)),
            dma((4, nt - 1)),
            dma((8,)),
        ],
        compiler_params=pltpu.CompilerParams(
            collective_id=0, has_side_effects=True, vmem_limit_bytes=60 * 2**20
        ),
    )(
        lambdas.T, query_first, query_second, norm_gain.reshape(1, feat), key_first, key_second,
        values.reshape(rows, -1), residual,
        out_weight.reshape(2 * value_size, model), gate_weight, up_weight, down_weight.T,
    )


def solution(mesh):
    return jax.shard_map(
        functools.partial(layer, mesh.shape["sp"] // 2, mesh.shape["tp"]),
        mesh=mesh,
        in_specs=(
            P(("grp", "sp"), "tp"),
            P(("grp", "sp"), "tp"),
            P(("grp", "sp"), "tp"),
            P(("grp", "sp"), "tp"),
            P(("grp", "sp"), None, "tp"),
            P(None, "tp"),
            P(("grp", "sp"), "tp"),
            P("tp"),
            P(None, "tp", None),
            P("sp", "tp"),
            P("sp", "tp"),
            P("tp", "sp"),
        ),
        out_specs=P(("grp", "sp"), "tp"),
        check_vma=False,
    )
```

time: 187 us -> 177 us (0.947); the launches traced: 184 us -> 176 us
  Pallas kernels: 179 us -> 172 us
    pallas_call x1, Pallas kernels: 179 us -> 172 us  [layer(): pl.pallas_call(functools.partial(kernel, nz, nt), out_shape=jax.ShapeDtyp...]
    unnamed x11 -> x4, local copies, waits for them, and re-layouts: 3.9 us -> 3.84 us
where the time goes in v2:
time: 177 us; the launch traced here: 176 us
  Pallas kernels  172 us (97%)
  local copies, waits for them, and re-layouts  4.41 us (2%)
    pallas_call x1, Pallas kernels, layer(): pl.pallas_call(functools.partial(kernel, nz, nt), out_shape=jax.ShapeDtyp...  172 us
    unnamed x4, local copies, waits for them, and re-layouts  3.84 us

profile of v2, /device:TPU:34, one launch (start us, length us, event | category | flops | bytes accessed | tf_op | source)
XLA Modules:
  0.0 176.1 jit_solution(9700973537863471066)
XLA Ops:
  0.0 0.0 copy-start
  0.0 0.7 copy-done
  0.7 0.6 reshape.9.gain_ref
  1.2 1.5 copy.15
  2.8 171.7 %shard_map.118 = bf16[192,512]{1,0:T(8,128)(2,1)} custom-call(f32[1,2]{1,0:T(1,128)} %bitcast.11, bf16[192,128]{1,0:T(8,128)(2,1)} %q1_ref.1, bf16[192,256]{1,0:T(8,128)(2,1)} %q2_ref.1, bf16[1,512]{1,0:T(2,128)(2,1)} %reshape.9.gain_ref, bf16[192,128]{1,0:T(8,128)(2,1)} %k1_hbm.1, bf16[192,256]{1,0:T(8,128)(2,1)} %k2_hbm.1, bf16[192,256]{1,0:T(8,128)(2,1)} %bitcast.8, ...), custom_call_target="tpu_custom_call" | custom-call | tf_op jit(solution)/shard_map/pallas_call | solution.py:479
  174.5 1.6 copy.17
Async XLA Ops:
  0.0 0.7 copy-start

commit v3 on v2

--- a/solution.py
+++ b/solution.py
@@ -13,6 +13,9 @@
 BF16 = jnp.bfloat16
 NT_DIMS = (((1,), (1,)), ((), ()))
 SPLIT = 16
+GATE_AT, DOWN_AT = 7, 9
+STREAM_AT, HIDDEN_AT = 12, 16
+ORDER = (2, 1, 3)
 
 
 class Ring:
@@ -143,19 +146,16 @@
         else:
             total(ring, 1 if count == 0 else count, dr.at[ring.index, d]).wait_recv()
 
-    def all_from_partner(rings):
-        for ring in rings:
-            from_partner(ring, 0, 0)
-
-            def step(d, carry):
-                from_partner(ring, d, 2)
-                return carry
-
-            lax.fori_loop(1, half, step, 0)
-            from_partner(ring, half, 1)
-
-    def turn(rings, then):
-        def step(d, carry):
+    def tick(rings, start, now):
+        d = now - start
+        if isinstance(start, int) and start > 0:
+
+            @pl.when(d == 0)
+            def _():
+                begin(rings)
+
+        @pl.when((d >= 1) & (d < half))
+        def _():
             for ring in rings:
                 for way in range(2):
                     landed(ring, way, d)
@@ -177,22 +177,38 @@
                 for ring in rings:
                     last_onward(ring).start()
 
-            then(d)
-            return carry
-
-        lax.fori_loop(1, half, step, 0)
-
-    def turn_end(rings):
-        for ring in rings:
-            landed(ring, 0, half)
-            pass_on(ring, 0, half)
-
-    def finish_across(rings):
-        for ring in rings:
-            if ring.across is not None:
-                for way in range(2):
-                    take_across(ring, way, half - 1)
-                take_across(ring, 0, half)
+        @pl.when(d == half)
+        def _():
+            for ring in rings:
+                landed(ring, 0, half)
+                pass_on(ring, 0, half)
+                if ring.across is not None:
+                    for way in range(2):
+                        take_across(ring, way, half - 1)
+
+        @pl.when(d == half + 1)
+        def _():
+            for ring in rings:
+                if ring.across is not None:
+                    take_across(ring, 0, half)
+
+    def gather(rings, start, now):
+        d = now - start
+
+        @pl.when(d == 1)
+        def _():
+            for ring in rings:
+                from_partner(ring, 0, 0)
+
+        @pl.when((d > 1) & (d <= half))
+        def _():
+            for ring in rings:
+                from_partner(ring, d - 1, 2)
+
+        @pl.when(d == half + 1)
+        def _():
+            for ring in rings:
+                from_partner(ring, half, 1)
 
     def all_sent(rings):
         for ring in rings:
@@ -289,79 +305,38 @@
     for load in loads[4:6]:
         load.wait()
 
-    def kv_then(d):
-        @pl.when(d == 1)
-        def _():
-            for ring in kv_rings:
-                from_partner(ring, 0, 0)
-            attend(z, True)
-
-        @pl.when(d == half - 2)
-        def _():
-            begin(gate_rings)
-
-        @pl.when(d > 1)
-        def _():
-            for ring in kv_rings:
-                from_partner(ring, d - 1, 2)
-            attend_step(d - 1)
-
-    turn(kv_rings + up_rings, kv_then)
-    turn_end(kv_rings + up_rings)
-    for ring in kv_rings:
-        from_partner(ring, half - 1, 2)
-    attend_step(half - 1)
-    for ring in kv_rings:
-        from_partner(ring, half, 1)
-
-    @pl.when(z >= half)
-    def _():
-        attend(z - half, False)
-
-    for group in range(2):
-        map_out = acc_ref[group] / l_ref[group]
-        differ = map_out[:rows] - lam_ref[0, group] * map_out[rows:]
-        scale = lax.rsqrt(jnp.mean(differ * differ, axis=1, keepdims=True) + 1e-06)
-        att[:, pl.ds(group * value_size, value_size)] = (0.8 * differ * scale).astype(BF16)
-    loads[6].wait()
-    order = (2, 1, 3)
-    for k in order:
-        cols = pl.ds(pl.multiple_of(feat * other(k), 128), feat)
-        mix_send[k - 1] = jnp.dot(att[...], ow[:, cols], preferred_element_type=F32).astype(BF16)
-    mix_own[...] = jnp.dot(
-        att[...], ow[:, pl.ds(pl.multiple_of(feat * t, 128), feat)], preferred_element_type=F32
-    )
-    for k in order:
-        mine(0, k).start()
-    loads[7].wait()
-
-    def gate_then(d):
-        @pl.when(d == 4)
-        def _():
-            acc = mix_own[...] + res[...].astype(F32)
-            for k in order:
-                theirs(0, k).wait_recv()
-                acc = acc + mix_recv[k - 1].astype(F32)
-            stream[...] = acc
-            sq[t] = jnp.broadcast_to(jnp.sum(acc * acc, axis=1, keepdims=True), sq.shape[1:])
-            xg[:, pl.ds(pl.multiple_of(feat * t, 128), feat)] = (
-                acc * gain_ref[...].astype(F32)
-            ).astype(BF16)
-            for k in order:
-                mine(1, k).start()
-                mine(2, k).start()
-
-        @pl.when(d == half - 2)
-        def _():
-            begin(down_rings)
-
-    finish_across(up_rings)
-    turn(gate_rings, gate_then)
-    turn_end(gate_rings)
-    all_from_partner(up_rings)
+    def project():
+        for group in range(2):
+            map_out = acc_ref[group] / l_ref[group]
+            differ = map_out[:rows] - lam_ref[0, group] * map_out[rows:]
+            scale = lax.rsqrt(jnp.mean(differ * differ, axis=1, keepdims=True) + 1e-06)
+            att[:, pl.ds(group * value_size, value_size)] = (0.8 * differ * scale).astype(BF16)
+        loads[6].wait()
+        for k in ORDER:
+            cols = pl.ds(pl.multiple_of(feat * other(k), 128), feat)
+            mix_send[k - 1] = jnp.dot(att[...], ow[:, cols], preferred_element_type=F32).astype(BF16)
+        mix_own[...] = jnp.dot(
+            att[...], ow[:, pl.ds(pl.multiple_of(feat * t, 128), feat)], preferred_element_type=F32
+        )
+        for k in ORDER:
+            mine(0, k).start()
+        loads[7].wait()
+
+    def make_stream():
+        acc = mix_own[...] + res[...].astype(F32)
+        for k in ORDER:
+            theirs(0, k).wait_recv()
+            acc = acc + mix_recv[k - 1].astype(F32)
+        stream[...] = acc
+        sq[t] = jnp.broadcast_to(jnp.sum(acc * acc, axis=1, keepdims=True), sq.shape[1:])
+        xg[:, pl.ds(pl.multiple_of(feat * t, 128), feat)] = (acc * gain_ref[...].astype(F32)).astype(BF16)
+        for k in ORDER:
+            mine(1, k).start()
+            mine(2, k).start()
 
     hidden = hid.shape[1]
     tile = 256
+    tiles, rest = hidden // tile, hidden % tile
 
     def hidden_tile(cols):
         scale = m_ref[0, pl.ds(0, rows), :][:, :1]
@@ -369,12 +344,8 @@
         ups = jnp.dot(xg[...], up[:, cols], preferred_element_type=F32) * scale
         hid[:, cols] = (gates / (1.0 + jnp.exp(-gates)) * ups).astype(BF16)
 
-    tiles, rest = hidden // tile, hidden % tile
-
     def hidden_units():
-        finish_across(gate_rings)
-        all_from_partner(gate_rings)
-        for k in order:
+        for k in ORDER:
             theirs(1, k).wait_recv()
             theirs(2, k).wait_recv()
         squares = sq[0]
@@ -389,66 +360,88 @@
         lax.fori_loop(0, tiles, one, 0)
         hidden_tile(pl.ds(tiles * tile, rest))
 
-    def share(owner):
-        parts = []
-        for i in range(2):
-            at = pl.ds(pl.multiple_of(feat * owner + i * (feat // 2), 16), feat // 2)
-            parts.append(lax.dot_general(hid[...], down[at, :], NT_DIMS, preferred_element_type=F32))
-        return jnp.concatenate(parts, axis=1)
-
-    def give(owner):
-        value = share(owner)
+    def give(zz):
+        width = 2 * wrows
+        owner = zz // (nz // nt)
+        cols = pl.ds(pl.multiple_of(width * lax.rem(zz, nz // nt), 128), width)
+        value = lax.dot_general(
+            hid[...], down[pl.ds(pl.multiple_of(width * zz, 16), width), :], NT_DIMS,
+            preferred_element_type=F32,
+        )
         k = lax.rem(owner - t + nt, nt)
 
         @pl.when(k == 0)
         def _():
-            ffn_own[...] = value
+            ffn_own[:, cols] = value
 
         @pl.when(k > 0)
         def _():
-            ffn_send[k - 1] = value.astype(BF16)
-            mine(3, k).start()
-
-    chips = nz // nt
-    here, place = z // chips, lax.rem(z, chips)
-
-    def near(v):
-        return lax.rem(here + v + nt, nt)
-
-    def down_then(d):
-        @pl.when(d == 1)
-        def _():
-            for ring in down_rings:
-                from_partner(ring, 0, 0)
-
-        @pl.when(d > 1)
-        def _():
-            for ring in down_rings:
-                from_partner(ring, d - 1, 2)
-
-        @pl.when(d == 2)
+            ffn_send[k - 1, :, cols] = value.astype(BF16)
+            swap(ffn_send.at[k - 1, :, cols], ffn_recv.at[k - 1, :, cols], 3, k).start()
+
+    def give_both(d):
+        def one(i, carry):
+            give(wrap(jnp.where(i == 0, z - d, z + d)))
+            return carry
+
+        lax.fori_loop(0, 2, one, 0)
+
+    last = DOWN_AT + half + 1
+
+    def all_steps(now, carry):
+        tick(kv_rings, 0, now)
+        tick(up_rings, 0, now)
+        tick(gate_rings, GATE_AT, now)
+        tick(down_rings, DOWN_AT, now)
+
+        gather(kv_rings, 0, now)
+
+        @pl.when(now == 1)
+        def _():
+            attend(z, True)
+
+        @pl.when((now > 1) & (now <= half))
+        def _():
+            attend_step(now - 1)
+
+        @pl.when(now == half + 1)
+        def _():
+            @pl.when(z >= half)
+            def _():
+                attend(z - half, False)
+
+            project()
+
+        @pl.when(now == STREAM_AT)
+        def _():
+            make_stream()
+
+        gather(up_rings, 1, now)
+        gather(gate_rings, GATE_AT, now)
+        gather(down_rings, DOWN_AT, now)
+
+        @pl.when(now == HIDDEN_AT)
         def _():
             hidden_units()
-
-        ready = (d == chips) | (d == chips + 1 + place) | (d == 2 * chips - place)
-
-        @pl.when(ready)
-        def _():
-            give(jnp.where(d == chips, here, jnp.where(d == chips + 1 + place, near(-1), near(1))))
-
-    turn(down_rings, down_then)
-    turn_end(down_rings)
-    finish_across(down_rings)
-    for ring in down_rings:
-        from_partner(ring, half - 1, 2)
-
-    @pl.when((place == 0) | (place == chips - 1))
-    def _():
-        give(jnp.where(place == 0, near(1), near(-1)))
-
-    for ring in down_rings:
-        from_partner(ring, half, 1)
-    give(near(2))
+            give(z)
+
+            def one(d, carry):
+                give_both(d)
+                return carry
+
+            lax.fori_loop(1, HIDDEN_AT - DOWN_AT, one, 0)
+
+        @pl.when((now > HIDDEN_AT) & (now < last))
+        def _():
+            give_both(now - 1 - DOWN_AT)
+
+        @pl.when(now == last)
+        def _():
+            give(wrap(z + half))
+
+        return carry
+
+    lax.fori_loop(1, last + 1, all_steps, 0)
     all_sent(kv_rings + up_rings + gate_rings + down_rings)
     for which in range(3):
         for k in range(1, nt):

time: 177 us -> 154 us (0.87)
  Pallas kernels: 172 us -> 149 us
    pallas_call x1, Pallas kernels: 172 us -> 149 us  [layer(): pl.pallas_call(functools.partial(kernel, nz, nt), out_shape=jax.ShapeDtyp...]
where the time goes in v3:
time: 154 us
  Pallas kernels  149 us (97%)
  local copies, waits for them, and re-layouts  4.41 us (3%)
    pallas_call x1, Pallas kernels, layer(): pl.pallas_call(functools.partial(kernel, nz, nt), out_shape=jax.ShapeDtyp...  149 us
    unnamed x4, local copies, waits for them, and re-layouts  3.84 us

profile of v3, /device:TPU:34, one launch (start us, length us, event | category | flops | bytes accessed | tf_op | source)
XLA Modules:
  0.0 153.6 jit_solution(9484460416030147045)
XLA Ops:
  0.0 0.0 copy-start
  0.0 0.7 copy-done
  0.7 0.6 reshape.9.gain_ref
  1.2 1.5 %copy.15 = bf16[24,8,2,128]{3,1,2,0:T(8,128)(2,1)} copy(bf16[24,8,2,128]{3,2,1,0:T(2,128)(2,1)} %bitcast.10) | data formatting | bytes 196608
  2.8 149.1 %shard_map.118 = bf16[192,512]{1,0:T(8,128)(2,1)} custom-call(f32[1,2]{1,0:T(1,128)} %bitcast.11, bf16[192,128]{1,0:T(8,128)(2,1)} %q1_ref.1, bf16[192,256]{1,0:T(8,128)(2,1)} %q2_ref.1, bf16[1,512]{1,0:T(2,128)(2,1)} %reshape.9.gain_ref, bf16[192,128]{1,0:T(8,128)(2,1)} %k1_hbm.1, bf16[192,256]{1,0:T(8,128)(2,1)} %k2_hbm.1, bf16[192,256]{1,0:T(8,128)(2,1)} %bitcast.8, ...), custom_call_target="tpu_custom_call" | custom-call | tf_op jit(solution)/shard_map/pallas_call | solution.py:472
  151.9 1.6 %copy.17 = bf16[192,512]{1,0:T(8,128)(2,1)} copy(bf16[192,512]{1,0:T(8,128)(2,1)} %shard_map.118) | data formatting | bytes 393216
Async XLA Ops:
  0.0 0.7 copy-start
